TPU v7x, 32 devices: a whole 2x2x4 slice. The times are simulated.
32 devices in a mesh: sp: 16 (over z, y, core), tp: 2 (over x).
Axes of the slice: x: 2, y: 2, z: 4, core: 2. Of those that a mesh axis runs over, the one named last changes fastest.
Arguments:
- tokens_in: bfloat16 [4096, 2048], P('sp', 'tp'), may hold values from -400 to 400
- norm_gain: float32 [2048], replicated, may hold values from 0.1 to 1.9
- w_query: bfloat16 [2048, 1024], P('sp', 'tp'), may hold values from -0.125 to 0.125
- w_forget: bfloat16 [2048, 1024], P('sp', 'tp'), may hold values from -0.125 to 0.125
- w_input: bfloat16 [2048, 1024], P('sp', 'tp'), may hold values from -0.125 to 0.125
- w_rgate: bfloat16 [2048, 1024], P('sp', 'tp'), may hold values from -0.125 to 0.125
- w_pool_in: bfloat16 [2048, 1024], P('sp', 'tp'), may hold values from -0.125 to 0.125
- w_pgate: bfloat16 [2048, 1024], P('sp', 'tp'), may hold values from -0.125 to 0.125
- floor_rate: float32 [1024], P('tp'), as said below
- extra_logdecay: float32 [4096, 8], P('sp', 'tp'), as said below
- state_gain: float32 [1024], P('tp'), may hold values from 0.1 to 1.9
- pool_mix: bfloat16 [8, 128, 128], P('tp'), may hold values from -0.5 to 0.5
- pool_gain: float32 [1024], P('tp'), may hold values from 0.1 to 1.9
- out_rec: bfloat16 [1024, 2048], P('tp', 'sp'), may hold values from -0.125 to 0.125
- out_pool: bfloat16 [1024, 2048], P('tp', 'sp'), may hold values from -0.125 to 0.125
- post_gain: float32 [2048], replicated, may hold values from 0.1 to 1.9
Outputs:
- mixed_out: bfloat16 [4096, 2048], P(('sp', 'tp'))
Inputs may be any that keep to these rules, and one draw needn't show every extreme that they name: `floor_rate`: every entry is positive. `extra_logdecay`: every entry is at most zero.
All inputs are finite; a program needn't handle non-finite values.
Results may differ from a plain program's by a relative error of at most 0.015.
Values may be sent and summed in bfloat16 or wider, within the bound.
A program may use at most 64 MiB of HBM per device.

v0:
```python
import jax
import jax.numpy as jnp
from jax import lax
from jax.sharding import PartitionSpec as P

DK = 128
BLOCK = 64
eps = 1e-06
coarsest_scale_depth = lax.Precision.HIGHEST


def prefix(part, axis, combine, identity):
    place = lax.axis_index(axis)
    gathered = jax.tree.map(lambda a: lax.all_gather(a, axis), part)
    state = jax.tree.map(lambda a, e: jnp.zeros_like(a) + jnp.asarray(e, a.dtype), part, identity)

    def one(turn, state):
        return combine(
            state, jax.tree.map(lambda a: lax.dynamic_index_in_dim(a, turn, 0, False), gathered)
        )

    return lax.fori_loop(0, place, one, state)


def shifted(value, axis, steps):
    count = lax.axis_size(axis)
    initial, last = (max(0, -steps), min(count, count - steps))
    return lax.ppermute(value, axis, [(source, source + steps) for source in range(initial, last)])


def chain_merge(earlier, later):
    return (earlier[0] * later[0], later[0][..., None] * earlier[1] + later[1])


def local_blocks(qs, keys, values, logs):
    causal = jnp.arange(BLOCK)[:, None] >= jnp.arange(BLOCK)[None, :]
    heads_dev = qs.shape[1]

    def advance(carry, member):
        carried_memory_matrix, start = carry
        probe_segment, key_piece, input_piece, gc = member
        prefix_sum_vector = jnp.cumsum(gc, axis=1)
        last_index = prefix_sum_vector[:, -1]
        cross_segment_contribution = jnp.einsum(
            "abz,azy->aby",
            probe_segment * jnp.exp(prefix_sum_vector),
            carried_memory_matrix,
            precision=coarsest_scale_depth,
        )
        diff = prefix_sum_vector[:, :, None, :] - prefix_sum_vector[:, None, :, :]
        weight = jnp.where(causal[None, :, :, None], jnp.exp(jnp.minimum(diff, 0.0)), 0.0)
        scores = jnp.einsum(
            "htk,hsk,htsk->hts", probe_segment, key_piece, weight, precision=coarsest_scale_depth
        )
        final_result = cross_segment_contribution + jnp.einsum(
            "hts,hsv->htv", scores, input_piece, precision=coarsest_scale_depth
        )
        carried_memory_matrix = jnp.exp(last_index)[..., None] * carried_memory_matrix + jnp.einsum(
            "njp,njq->npq",
            key_piece * jnp.exp(last_index[:, None, :] - prefix_sum_vector),
            input_piece,
            precision=coarsest_scale_depth,
        )
        pool_reach = probe_segment * jnp.exp(start[:, None, :] + prefix_sum_vector)
        return ((carried_memory_matrix, start + last_index), (final_result, pool_reach))

    begin = (jnp.zeros((heads_dev, DK, DK), jnp.float32), jnp.zeros((heads_dev, DK), jnp.float32))
    (carried_memory_matrix, total), (final_result, pool_reach) = lax.scan(
        advance, begin, (qs, keys, values, logs)
    )
    return (carried_memory_matrix, total, final_result, pool_reach)


def per_device(
    tokens_in,
    norm_gain,
    w_query,
    w_forget,
    w_input,
    w_rgate,
    w_pool_in,
    w_pgate,
    floor_rate,
    extra_logdecay,
    state_gain,
    pool_mix,
    pool_gain,
    out_rec,
    out_pool,
    post_gain,
):
    gathered = (
        lax.all_gather(w_query, "sp", axis=0, tiled=True),
        lax.all_gather(w_forget, "sp", axis=0, tiled=True),
        lax.all_gather(w_input, "sp", axis=0, tiled=True),
        lax.all_gather(w_rgate, "sp", axis=0, tiled=True),
        lax.all_gather(w_pool_in, "sp", axis=0, tiled=True),
        lax.all_gather(w_pgate, "sp", axis=0, tiled=True),
    )
    joined = jnp.concatenate(gathered, axis=1)
    head_cols = w_query.shape[1]
    positions = tokens_in.shape[0]
    model_width = norm_gain.shape[0]
    wide = lax.all_gather(tokens_in, "tp", axis=1, tiled=True).astype(jnp.float32)
    scaled = (wide * norm_gain[None, :]).astype(jnp.bfloat16)
    totals = jnp.dot(scaled, joined, preferred_element_type=jnp.float32)
    squares = jnp.sum(wide * wide, axis=1)
    inv_rms = lax.rsqrt(squares / model_width + eps)
    proj = (totals * inv_rms[:, None]).astype(jnp.bfloat16)
    query = proj[:, 0:head_cols]
    forget = proj[:, head_cols : 2 * head_cols]
    inputs = proj[:, 2 * head_cols : 3 * head_cols]
    rgate = proj[:, 3 * head_cols : 4 * head_cols]
    pool_in = proj[:, 4 * head_cols : 5 * head_cols]
    pgate = proj[:, 5 * head_cols : 6 * head_cols]
    heads_dev = head_cols // DK
    blocks = positions // BLOCK

    def to_blocks(array):
        return array.reshape(blocks, BLOCK, heads_dev, DK).transpose(0, 2, 1, 3)

    forget32 = forget.astype(jnp.float32)
    key_gate = -jnp.expm1(-floor_rate)[None, :] * jax.nn.sigmoid(-forget32)
    log_forget = jnp.log1p(-key_gate) + jnp.repeat(extra_logdecay, DK, axis=1)
    qs = query.astype(jnp.float32) * DK ** (-0.5)
    carried_memory_matrix, total, final_result, pool_reach = local_blocks(
        to_blocks(qs),
        to_blocks(key_gate),
        to_blocks(inputs.astype(jnp.float32)),
        to_blocks(log_forget),
    )
    decays = jnp.exp(total)
    tail_rows = pool_in[positions - 16 :]
    carried = prefix(
        (decays, carried_memory_matrix),
        "sp",
        chain_merge,
        (jnp.ones_like(decays), jnp.zeros_like(carried_memory_matrix)),
    )
    incoming_state = carried[1]
    previous = shifted(tail_rows, "sp", 1).astype(jnp.float32)
    recurrent_output = final_result + jnp.einsum(
        "izaf,zfu->izau", pool_reach, incoming_state, precision=coarsest_scale_depth
    )
    grouped = recurrent_output.transpose(0, 2, 1, 3).reshape(positions, heads_dev, DK)
    normed = grouped * lax.rsqrt(jnp.mean(grouped * grouped, axis=2, keepdims=True) + eps)
    y_rec = (
        normed.reshape(positions, head_cols)
        * state_gain[None, :]
        * jax.nn.silu(rgate.astype(jnp.float32))
    ).astype(jnp.bfloat16)
    group = lax.axis_index("tp") * heads_dev + jnp.arange(head_cols) // DK
    window = jnp.power(2, 1 + group % 4).astype(jnp.int32)
    pool32 = pool_in.astype(jnp.float32)
    extended = jnp.concatenate([previous, pool32], axis=0)
    summed_rows = jnp.zeros((positions, head_cols), jnp.float32)
    for offset in range(16):
        rows_back = extended[16 - offset : 16 - offset + positions]
        summed_rows = summed_rows + jnp.where((offset < window)[None, :], rows_back, 0.0)
    place = lax.axis_index("sp") * positions + jnp.arange(positions)
    count = jnp.minimum(place[:, None] + 1, window[None, :]).astype(jnp.float32)
    mixed = (summed_rows / count - pool32).astype(jnp.bfloat16)
    mapped = jnp.einsum(
        "tgc,gcd->tgd",
        mixed.reshape(positions, heads_dev, DK),
        pool_mix,
        preferred_element_type=jnp.float32,
    ).reshape(positions, head_cols)
    y_pool = (mapped * pool_gain[None, :] * jax.nn.silu(pgate.astype(jnp.float32))).astype(
        jnp.bfloat16
    )
    out_parts = (
        lax.all_gather(out_rec, "sp", axis=1, tiled=True),
        lax.all_gather(out_pool, "sp", axis=1, tiled=True),
    )
    both = jnp.concatenate([y_rec, y_pool], axis=1)
    weight_cat = jnp.concatenate(out_parts, axis=0)
    summed = lax.psum_scatter(
        jnp.dot(both, weight_cat, preferred_element_type=jnp.float32).astype(jnp.bfloat16),
        "tp",
        scatter_dimension=0,
        tiled=True,
    ).astype(jnp.float32)
    final = (
        summed
        * lax.rsqrt(jnp.mean(summed * summed, axis=1, keepdims=True) + eps)
        * post_gain[None, :]
    )
    return final.astype(jnp.bfloat16)


def solution(mesh):
    placed = (
        P("sp", "tp"),
        P(),
        P("sp", "tp"),
        P("sp", "tp"),
        P("sp", "tp"),
        P("sp", "tp"),
        P("sp", "tp"),
        P("sp", "tp"),
        P("tp"),
        P("sp", "tp"),
        P("tp"),
        P("tp", None, None),
        P("tp"),
        P("tp", "sp"),
        P("tp", "sp"),
        P(),
    )
    return jax.shard_map(
        per_device, mesh=mesh, in_specs=placed, out_specs=P(("sp", "tp"), None), check_vma=False
    )
```

profile of v0, /device:TPU:0, one launch (start us, length us, event | category | flops | bytes accessed | tf_op | source)
XLA Modules:
  0.0 518.1 jit_solution(14276728240443677830)
XLA Ops:
  12.8 20.1 %all-gather.14.cloned.1.call-done = bf16[256,2048]{1,0:T(8,128)(2,1)} async-done(((bf16[256,1024]{1,0:T(8,128)(2,1)}), bf16[256,2048]{1,0:T(8,128)(2,1)}) %all-gather.14.cloned.1.call-update) | async-done | bytes 1048592 | tf_op jit(solution)/shard_map/all_gather | solution.py:104
  34.4 42.1 %all-gather.16.cloned.1.call-done = bf16[2048,512]{1,0:T(8,128)(2,1)} async-done(((bf16[128,512]{1,0:T(8,128)(2,1)}), bf16[2048,512]{1,0:T(8,128)(2,1)}) %all-gather.16.cloned.1.call-update) | async-done | bytes 2097168 | tf_op jit(solution)/shard_map/all_gather | solution.py:93
  76.6 3.2 constant_dynamic-update-slice_fusion.5
  79.7 39.2 %all-gather.18.cloned.1.call-done = bf16[2048,512]{1,0:T(8,128)(2,1)} async-done(((bf16[128,512]{1,0:T(8,128)(2,1)}), bf16[2048,512]{1,0:T(8,128)(2,1)}) %all-gather.18.cloned.1.call-update) | async-done | bytes 2097168 | tf_op jit(solution)/shard_map/all_gather | solution.py:94
  118.9 3.2 constant_dynamic-update-slice_fusion.4
  122.2 39.0 %all-gather.20.cloned.1.call-done = bf16[2048,512]{1,0:T(8,128)(2,1)} async-done(((bf16[128,512]{1,0:T(8,128)(2,1)}), bf16[2048,512]{1,0:T(8,128)(2,1)}) %all-gather.20.cloned.1.call-update) | async-done | bytes 2097168 | tf_op jit(solution)/shard_map/all_gather | solution.py:95
  161.2 3.1 constant_dynamic-update-slice_fusion.3
  164.3 39.1 %all-gather.22.cloned.1.call-done = bf16[2048,512]{1,0:T(8,128)(2,1)} async-done(((bf16[128,512]{1,0:T(8,128)(2,1)}), bf16[2048,512]{1,0:T(8,128)(2,1)}) %all-gather.22.cloned.1.call-update) | async-done | bytes 2097168 | tf_op jit(solution)/shard_map/all_gather | solution.py:96
  203.4 3.2 constant_dynamic-update-slice_fusion.2
  206.6 39.0 %all-gather.24.cloned.1.call-done = bf16[2048,512]{1,0:T(8,128)(2,1)} async-done(((bf16[128,512]{1,0:T(8,128)(2,1)}), bf16[2048,512]{1,0:T(8,128)(2,1)}) %all-gather.24.cloned.1.call-update) | async-done | bytes 2097168 | tf_op jit(solution)/shard_map/all_gather | solution.py:97
  245.6 3.2 constant_dynamic-update-slice_fusion.1
  248.8 39.1 %all-gather.26.cloned.1.call-done = bf16[2048,512]{1,0:T(8,128)(2,1)} async-done(((bf16[128,512]{1,0:T(8,128)(2,1)}), bf16[2048,512]{1,0:T(8,128)(2,1)}) %all-gather.26.cloned.1.call-update) | async-done | bytes 2097168 | tf_op jit(solution)/shard_map/all_gather | solution.py:98
  288.0 3.1 constant_dynamic-update-slice_fusion
  291.1 8.0 %fusion.29 = bf16[256,3072]{1,0:T(8,128)(2,1)S(1)} fusion(bf16[2048,3072]{1,0:T(8,128)(2,1)} %constant_dynamic-update-slice_fusion, f32[256]{0:T(256)S(1)} %add_rsqrt_fusion.1, bf16[256,2048]{1,0:T(8,128)(2,1)S(1)} %copy-done.3, f32[2048]{0:T(1024)S(1)} %copy-done.10), kind=kOutput, calls=%fused_computation.44 | convolution fusion | flops 3224371200 | bytes 15213568 | tf_op jit(solution)/shard_map/dot_general | solution.py:106
  301.9 48.2 %while.30 = (s32[]{:T(128)}, f32[4,128,128]{2,1,0:T(8,128)S(1)}, f32[4,128]{1,0:T(4,128)S(1)}, f32[4,4,64,128]{3,2,0,1:T(8,128)}, f32[4,4,64,128]{3,2,0,1:T(8,12...) while((s32[]{:T(128)}, f32[4,128,128]{2,1,0:T(8,128)S(1)}, ...), condition=%wide.region_3.4_spmd.clone, body=%wide.region_1.3_spmd.clone.sunk | while | flops 140923904 | bytes 20806288 | solution.py:68
  302.3 1.7 exponential_select_fusion.2
  304.0 7.3 %fusion.136 = f32[4,64,64]{1,2,0:T(8,128)S(1)} fusion(f32[4,64,64,128]{3,2,1,0:T(8,128)S(1)} %exponential_select_fusion.2, f32[4,128,64]{1,2,0:T(8,128)S(1)} %dynamic-slice_bitcast_fusion.9, f32[4,128,64]{1,2,0:T(8,128)S(1)} %get-tuple-element.298), kind=kLoop, calls=%fused_computation.4.clone.1 | loop fusion | flops 6275072 | bytes 8716288 | tf_op jit(solution)/shard_map/while/body/eval_jaxpr/htk,hsk,htsk->hts/dot_general | solution.py:52
  314.3 1.7 exponential_select_fusion.2
  316.0 7.3 %fusion.136 = f32[4,64,64]{1,2,0:T(8,128)S(1)} fusion(f32[4,64,64,128]{3,2,1,0:T(8,128)S(1)} %exponential_select_fusion.2, f32[4,128,64]{1,2,0:T(8,128)S(1)} %dynamic-slice_bitcast_fusion.9, f32[4,128,64]{1,2,0:T(8,128)S(1)} %get-tuple-element.298), kind=kLoop, calls=%fused_computation.4.clone.1 | loop fusion | flops 6275072 | bytes 8716288 | tf_op jit(solution)/shard_map/while/body/eval_jaxpr/htk,hsk,htsk->hts/dot_general | solution.py:52
  326.3 1.7 exponential_select_fusion.2
  328.0 7.3 %fusion.136 = f32[4,64,64]{1,2,0:T(8,128)S(1)} fusion(f32[4,64,64,128]{3,2,1,0:T(8,128)S(1)} %exponential_select_fusion.2, f32[4,128,64]{1,2,0:T(8,128)S(1)} %dynamic-slice_bitcast_fusion.9, f32[4,128,64]{1,2,0:T(8,128)S(1)} %get-tuple-element.298), kind=kLoop, calls=%fused_computation.4.clone.1 | loop fusion | flops 6275072 | bytes 8716288 | tf_op jit(solution)/shard_map/while/body/eval_jaxpr/htk,hsk,htsk->hts/dot_general | solution.py:52
  338.3 1.7 exponential_select_fusion.2
  340.0 7.3 %fusion.136 = f32[4,64,64]{1,2,0:T(8,128)S(1)} fusion(f32[4,64,64,128]{3,2,1,0:T(8,128)S(1)} %exponential_select_fusion.2, f32[4,128,64]{1,2,0:T(8,128)S(1)} %dynamic-slice_bitcast_fusion.9, f32[4,128,64]{1,2,0:T(8,128)S(1)} %get-tuple-element.298), kind=kLoop, calls=%fused_computation.4.clone.1 | loop fusion | flops 6275072 | bytes 8716288 | tf_op jit(solution)/shard_map/while/body/eval_jaxpr/htk,hsk,htsk->hts/dot_general | solution.py:52
  353.2 2.1 collective-permute-start
  355.4 19.7 %all-gather.2 = f32[16,4,128]{2,1,0:T(4,128)S(1)} all-gather(f32[1,4,128]{2,1,0:T(4,128)S(1)} %exponential_bitcast_fusion), channel_id=2, replica_groups=mesh['sp'=16,'tp'=2] {'sp'}, dimensions={0}, use_global_device_ids=true | all-gather | bytes 34816 | tf_op jit(solution)/shard_map/all_gather | solution.py:14
  375.1 1.7 fusion.103
  377.0 23.2 %all-gather.32.cloned.1.call-done = f32[64,128,128]{2,1,0:T(8,128)} async-done(((f32[4,128,128]{2,1,0:T(8,128)}), f32[64,128,128]{2,1,0:T(8,128)}) %all-gather.32.cloned.1.call-update) | async-done | bytes 4194320 | tf_op jit(solution)/shard_map/all_gather | solution.py:14
  403.2 38.8 %all-gather.28.cloned.1.call-done = bf16[512,2048]{1,0:T(8,128)(2,1)} async-done(((bf16[512,128]{1,0:T(8,128)(2,1)}), bf16[512,2048]{1,0:T(8,128)(2,1)}) %all-gather.28.cloned.1.call-update) | async-done | bytes 2097168 | tf_op jit(solution)/shard_map/all_gather | solution.py:173
  442.0 42.2 %all-gather.30.cloned.1.call-done = bf16[512,2048]{1,0:T(8,128)(2,1)} async-done(((bf16[512,128]{1,0:T(8,128)(2,1)}), bf16[512,2048]{1,0:T(8,128)(2,1)}) %all-gather.30.cloned.1.call-update) | async-done | bytes 2097168 | tf_op jit(solution)/shard_map/all_gather | solution.py:174
  484.1 4.5 fusion.30
  488.6 19.6 %reduce-scatter.2.cloned.1.call-done = bf16[128,2048]{1,0:T(8,128)(2,1)} async-done(((bf16[256,2048]{1,0:T(8,128)(2,1)}), bf16[128,2048]{1,0:T(8,128)(2,1)}) %reduce-scatter.2.cloned.1.call-update) | async-done | bytes 524304 | tf_op jit(solution)/shard_map/reduce_scatter | solution.py:178
  509.5 2.0 fusion.39
  (126 shorter events, 29.7 us)
Async XLA Ops:
  6.5 368.5 %copy-start = (bf16[4,128,128]{2,1,0:T(8,128)(2,1)S(1)}, bf16[4,128,128]{2,1,0:T(8,128)(2,1)}, u32[]{:S(2)}) copy-start(bf16[4,128,128]{2,1,0:T(8,128)(2,1)} %param.31) | copy-start | bytes 393220
  6.5 26.4 %all-gather.14.cloned.1.call-start = ((), (), s32[]{:S(2)}) async-start(), calls=%async_computation.1 | async-start | bytes 1572864 | tf_op jit(solution)/shard_map/all_gather | solution.py:104
  7.3 69.3 %all-gather.16.cloned.1.call-start = ((), (), s32[]{:S(2)}) async-start(), calls=%async_computation.2 | async-start | bytes 2228224 | tf_op jit(solution)/shard_map/all_gather | solution.py:93
  8.0 110.9 %all-gather.18.cloned.1.call-start = ((), (), s32[]{:S(2)}) async-start(), calls=%async_computation.3 | async-start | bytes 2228224 | tf_op jit(solution)/shard_map/all_gather | solution.py:94
  8.7 152.4 %all-gather.20.cloned.1.call-start = ((), (), s32[]{:S(2)}) async-start(), calls=%async_computation.4 | async-start | bytes 2228224 | tf_op jit(solution)/shard_map/all_gather | solution.py:95
  9.3 194.1 %all-gather.22.cloned.1.call-start = ((), (), s32[]{:S(2)}) async-start(), calls=%async_computation.5 | async-start | bytes 2228224 | tf_op jit(solution)/shard_map/all_gather | solution.py:96
  9.9 235.7 %all-gather.24.cloned.1.call-start = ((), (), s32[]{:S(2)}) async-start(), calls=%async_computation.6 | async-start | bytes 2228224 | tf_op jit(solution)/shard_map/all_gather | solution.py:97
  10.5 277.5 %all-gather.26.cloned.1.call-start = ((), (), s32[]{:S(2)}) async-start(), calls=%async_computation.7 | async-start | bytes 2228224 | tf_op jit(solution)/shard_map/all_gather | solution.py:98
  11.2 389.0 %all-gather.32.cloned.1.call-start = ((), (), s32[]{:S(2)}) async-start(), calls=%async_computation.11 | async-start | bytes 4456448 | tf_op jit(solution)/shard_map/all_gather | solution.py:14
  206.6 84.5 %copy-start.3 = (bf16[256,2048]{1,0:T(8,128)(2,1)S(1)}, bf16[256,2048]{1,0:T(8,128)(2,1)}, u32[]{:S(2)}) copy-start(bf16[256,2048]{1,0:T(8,128)(2,1)} %all-gather.14.cloned.1.call-done) | copy-start | bytes 3145732
  206.6 84.5 %copy-start.10 = (f32[2048]{0:T(1024)S(1)}, f32[2048]{0:T(1024)}, u32[]{:S(2)}) copy-start(f32[2048]{0:T(1024)} %param.21) | copy-start | bytes 24580
  299.1 1.7 copy-start.2
  301.9 73.2 %copy-start.4 = (f32[256,512]{1,0:T(8,128)S(1)}, f32[256,512]{1,0:T(8,128)}, u32[]{:S(2)}) copy-start(f32[256,512]{1,0:T(8,128)} %get-tuple-element.180) | copy-start | bytes 1572868
  350.1 0.7 copy-start.1
  350.9 91.1 %all-gather.28.cloned.1.call-start = ((), (), s32[]{:S(2)}) async-start(), calls=%async_computation.8 | async-start | bytes 2228224 | tf_op jit(solution)/shard_map/all_gather | solution.py:173
  351.6 132.5 %all-gather.30.cloned.1.call-start = ((), (), s32[]{:S(2)}) async-start(), calls=%async_computation.9 | async-start | bytes 2228224 | tf_op jit(solution)/shard_map/all_gather | solution.py:174
  352.2 156.1 %reduce-scatter.2.cloned.1.call-start = ((), (), s32[]{:S(2)}) async-start(), calls=%async_computation.10 | async-start | bytes 1572864 | tf_op jit(solution)/shard_map/reduce_scatter | solution.py:178
  353.2 21.8 %collective-permute-start = (bf16[16,512]{1,0:T(8,128)(2,1)S(1)}, bf16[16,512]{1,0:T(8,128)(2,1)S(1)}, u32[]{:S(2)}, u32[]{:S(2)}) collective-permute-start(bf16[16,512]{1,0:T(8,128)(2,1)S(1)} %slice.99), channel_id=1, source_target_pairs={{0,2},{2,4},{4,6},{6,8},{8,10},{10,12},{12,14},{14,16},{16,18},{18... | collective-permute-start | bytes 49160 | tf_op jit(solution)/shard_map/ppermute | solution.py:28
  376.8 23.4 %copy-start.5 = (f32[4,4,64,128]{3,2,0,1:T(8,128)S(1)}, f32[4,4,64,128]{3,2,0,1:T(8,128)}, u32[]{:S(2)}) copy-start(f32[4,4,64,128]{3,2,0,1:T(8,128)} %get-tuple-element.104) | copy-start | bytes 1572868
  376.8 23.4 %copy-start.6 = (f32[4,4,64,128]{3,2,0,1:T(8,128)S(1)}, f32[4,4,64,128]{3,2,0,1:T(8,128)}, u32[]{:S(2)}) copy-start(f32[4,4,64,128]{3,2,0,1:T(8,128)} %get-tuple-element.108) | copy-start | bytes 1572868
  377.0 24.8 %copy-start.8 = (f32[512]{0:T(512)S(1)}, f32[512]{0:T(512)}, u32[]{:S(2)}) copy-start(f32[512]{0:T(512)} %param.30) | copy-start | bytes 6148
  377.0 24.8 %copy-start.9 = (f32[512]{0:T(512)S(1)}, f32[512]{0:T(512)}, u32[]{:S(2)}) copy-start(f32[512]{0:T(512)} %param.32) | copy-start | bytes 6148
  484.1 25.4 %copy-start.7 = (f32[2048]{0:T(1024)S(1)}, f32[2048]{0:T(1024)}, u32[]{:S(2)}) copy-start(f32[2048]{0:T(1024)} %param.35) | copy-start | bytes 24580
Sparse Core Ops, SparseCore 0:
  8.9 23.9 all-gather.13
  35.1 41.4 all-gather.15
  78.7 40.1 all-gather.17
  121.0 40.1 all-gather.19
  163.2 40.1 all-gather.21
  205.4 40.1 all-gather.23
  247.8 40.1 all-gather.25
  351.0 49.1 all-gather.31
  402.4 39.5 all-gather.27
  444.0 40.1 all-gather.29
  488.8 19.4 reduce-scatter.1
where the time goes:
time: 519 us; the launch traced here: 518 us
  waiting for transfers between devices  387 us (75%)
  other arithmetic  47.9 us (9%)
  local copies, waits for them, and re-layouts  23.9 us (5%)
  matrix products  23.2 us (4%)
  blocking collectives  19.7 us (4%)
  between operations  13.6 us (3%)
    all_gather x1, waiting for transfers between devices, per_device(): lax.all_gather(out_pool, 'sp', axis=1, tiled=True)  42.2 us
    all_gather x1, waiting for transfers between devices, per_device(): lax.all_gather(w_query, 'sp', axis=0, tiled=True)  42.1 us
    all_gather x1, waiting for transfers between devices, per_device(): lax.all_gather(w_forget, 'sp', axis=0, tiled=True)  39.2 us
    all_gather x1, waiting for transfers between devices, per_device(): lax.all_gather(w_pgate, 'sp', axis=0, tiled=True)  39.1 us
    all_gather x1, waiting for transfers between devices, per_device(): lax.all_gather(w_rgate, 'sp', axis=0, tiled=True)  39.1 us
    all_gather x1, waiting for transfers between devices, per_device(): lax.all_gather(w_pool_in, 'sp', axis=0, tiled=True)  39 us
    all_gather x1, waiting for transfers between devices, per_device(): lax.all_gather(w_input, 'sp', axis=0, tiled=True)  39 us
    all_gather x1, waiting for transfers between devices, per_device(): lax.all_gather(out_rec, 'sp', axis=1, tiled=True)  38.8 us
  transfers between devices with their start and end apart: 12, of which 11 were waited for; matrix products, arithmetic and copies ran while one was open for 5% of the time, Pallas kernels for 0%

commit v1 on v0

--- a/solution.py
+++ b/solution.py
@@ -7,6 +7,11 @@
 BLOCK = 64
 eps = 1e-06
 coarsest_scale_depth = lax.Precision.HIGHEST
+
+
+def remake_spots_now(u_in, axis_key):
+    all_values = jnp.concatenate(lax.all_gather(u_in, axis_key), axis=1)
+    return all_values
 
 
 def prefix(part, axis, combine, identity):
@@ -170,7 +175,7 @@
         jnp.bfloat16
     )
     out_parts = (
-        lax.all_gather(out_rec, "sp", axis=1, tiled=True),
+        remake_spots_now(out_rec, "sp"),
         lax.all_gather(out_pool, "sp", axis=1, tiled=True),
     )
     both = jnp.concatenate([y_rec, y_pool], axis=1)

time: 519 us -> 476 us (0.917)
  waiting for transfers between devices: 387 us -> 340 us
    all_gather x1, waiting for transfers between devices: 38.8 us -> 0.02 us  [remake_spots_now(): all_values = jnp.concatenate(lax.all_gather(u_in, axis_key), axis=1)]
    unnamed x29 -> x26, local copies, waits for them, and re-layouts: 17.6 us -> 18 us
  transfers between devices with their start and end apart: 12 -> 12, of which waited for: 11 -> 10; matrix products, arithmetic and copies ran while one was open for 5% -> 19% of each run, Pallas kernels for 0% -> 0%
where the time goes in v1:
time: 476 us; the launch traced here: 475 us
  waiting for transfers between devices  340 us (71%)
  other arithmetic  47.9 us (10%)
  local copies, waits for them, and re-layouts  27.5 us (6%)
  matrix products  23.8 us (5%)
  blocking collectives  19.4 us (4%)
  between operations  13.5 us (3%)
    all_gather x1, waiting for transfers between devices, per_device(): lax.all_gather(w_query, 'sp', axis=0, tiled=True)  42.1 us
    all_gather x1, waiting for transfers between devices, per_device(): lax.all_gather(w_forget, 'sp', axis=0, tiled=True)  39.2 us
    all_gather x1, waiting for transfers between devices, per_device(): lax.all_gather(w_pgate, 'sp', axis=0, tiled=True)  39.2 us
    all_gather x1, waiting for transfers between devices, per_device(): lax.all_gather(w_pool_in, 'sp', axis=0, tiled=True)  39.1 us
    all_gather x1, waiting for transfers between devices, per_device(): lax.all_gather(w_input, 'sp', axis=0, tiled=True)  39 us
    all_gather x1, waiting for transfers between devices, per_device(): lax.all_gather(w_rgate, 'sp', axis=0, tiled=True)  39 us
    all_gather x1, waiting for transfers between devices, per_device(): lax.all_gather(out_pool, 'sp', axis=1, tiled=True)  37.4 us
    dot_general x4, other arithmetic, advance(): jnp.einsum('htk,hsk,htsk->hts', probe_segment, key_piece, weight, precisi...  29.3 us
  transfers between devices with their start and end apart: 12, of which 10 were waited for; matrix products, arithmetic and copies ran while one was open for 19% of the time, Pallas kernels for 0%

profile of v1, /device:TPU:0, one launch (start us, length us, event | category | flops | bytes accessed | tf_op | source)
XLA Modules:
  0.0 475.2 jit_solution(4810586418535087580)
XLA Ops:
  13.6 19.3 %all-gather.15.cloned.1.call-done = bf16[256,2048]{1,0:T(8,128)(2,1)} async-done(((bf16[256,1024]{1,0:T(8,128)(2,1)}), bf16[256,2048]{1,0:T(8,128)(2,1)}) %all-gather.15.cloned.1.call-update) | async-done | bytes 1048592 | tf_op jit(solution)/shard_map/all_gather | solution.py:109
  34.4 42.1 %all-gather.17.cloned.1.call-done = bf16[2048,512]{1,0:T(8,128)(2,1)} async-done(((bf16[128,512]{1,0:T(8,128)(2,1)}), bf16[2048,512]{1,0:T(8,128)(2,1)}) %all-gather.17.cloned.1.call-update) | async-done | bytes 2097168 | tf_op jit(solution)/shard_map/all_gather | solution.py:98
  76.6 3.1 constant_dynamic-update-slice_fusion.5
  79.7 39.2 %all-gather.19.cloned.1.call-done = bf16[2048,512]{1,0:T(8,128)(2,1)} async-done(((bf16[128,512]{1,0:T(8,128)(2,1)}), bf16[2048,512]{1,0:T(8,128)(2,1)}) %all-gather.19.cloned.1.call-update) | async-done | bytes 2097168 | tf_op jit(solution)/shard_map/all_gather | solution.py:99
  118.9 3.2 constant_dynamic-update-slice_fusion.4
  122.1 39.0 %all-gather.21.cloned.1.call-done = bf16[2048,512]{1,0:T(8,128)(2,1)} async-done(((bf16[128,512]{1,0:T(8,128)(2,1)}), bf16[2048,512]{1,0:T(8,128)(2,1)}) %all-gather.21.cloned.1.call-update) | async-done | bytes 2097168 | tf_op jit(solution)/shard_map/all_gather | solution.py:100
  161.2 3.2 constant_dynamic-update-slice_fusion.3
  164.4 39.0 %all-gather.23.cloned.1.call-done = bf16[2048,512]{1,0:T(8,128)(2,1)} async-done(((bf16[128,512]{1,0:T(8,128)(2,1)}), bf16[2048,512]{1,0:T(8,128)(2,1)}) %all-gather.23.cloned.1.call-update) | async-done | bytes 2097168 | tf_op jit(solution)/shard_map/all_gather | solution.py:101
  203.4 3.1 constant_dynamic-update-slice_fusion.2
  206.5 39.1 %all-gather.25.cloned.1.call-done = bf16[2048,512]{1,0:T(8,128)(2,1)} async-done(((bf16[128,512]{1,0:T(8,128)(2,1)}), bf16[2048,512]{1,0:T(8,128)(2,1)}) %all-gather.25.cloned.1.call-update) | async-done | bytes 2097168 | tf_op jit(solution)/shard_map/all_gather | solution.py:102
  245.6 3.2 constant_dynamic-update-slice_fusion.1
  248.8 39.2 %all-gather.27.cloned.1.call-done = bf16[2048,512]{1,0:T(8,128)(2,1)} async-done(((bf16[128,512]{1,0:T(8,128)(2,1)}), bf16[2048,512]{1,0:T(8,128)(2,1)}) %all-gather.27.cloned.1.call-update) | async-done | bytes 2097168 | tf_op jit(solution)/shard_map/all_gather | solution.py:103
  288.0 3.2 constant_dynamic-update-slice_fusion
  291.2 8.0 %fusion.29 = bf16[256,3072]{1,0:T(8,128)(2,1)S(1)} fusion(bf16[2048,3072]{1,0:T(8,128)(2,1)} %constant_dynamic-update-slice_fusion, f32[256]{0:T(256)S(1)} %add_rsqrt_fusion.1, bf16[256,2048]{1,0:T(8,128)(2,1)S(1)} %copy-done.3, f32[2048]{0:T(1024)S(1)} %copy-done.8), kind=kOutput, calls=%fused_computation.44 | convolution fusion | flops 3224371200 | bytes 15213568 | tf_op jit(solution)/shard_map/dot_general | solution.py:111
  302.0 48.3 %while.30 = (s32[]{:T(128)}, f32[4,128,128]{2,1,0:T(8,128)S(1)}, f32[4,128]{1,0:T(4,128)S(1)}, f32[4,4,64,128]{3,2,0,1:T(8,128)}, f32[4,4,64,128]{3,2,0,1:T(8,12...) while((s32[]{:T(128)}, f32[4,128,128]{2,1,0:T(8,128)S(1)}, ...), condition=%wide.region_3.4_spmd.clone, body=%wide.region_1.3_spmd.clone.sunk | while | flops 140923904 | bytes 20806288 | solution.py:73
  302.4 1.7 exponential_select_fusion.2
  304.1 7.3 %fusion.136 = f32[4,64,64]{1,2,0:T(8,128)S(1)} fusion(f32[4,64,64,128]{3,2,1,0:T(8,128)S(1)} %exponential_select_fusion.2, f32[4,128,64]{1,2,0:T(8,128)S(1)} %dynamic-slice_bitcast_fusion.9, f32[4,128,64]{1,2,0:T(8,128)S(1)} %get-tuple-element.298), kind=kLoop, calls=%fused_computation.4.clone.1 | loop fusion | flops 6275072 | bytes 8716288 | tf_op jit(solution)/shard_map/while/body/eval_jaxpr/htk,hsk,htsk->hts/dot_general | solution.py:57
  316.1 7.3 %fusion.136 = f32[4,64,64]{1,2,0:T(8,128)S(1)} fusion(f32[4,64,64,128]{3,2,1,0:T(8,128)S(1)} %exponential_select_fusion.2, f32[4,128,64]{1,2,0:T(8,128)S(1)} %dynamic-slice_bitcast_fusion.9, f32[4,128,64]{1,2,0:T(8,128)S(1)} %get-tuple-element.298), kind=kLoop, calls=%fused_computation.4.clone.1 | loop fusion | flops 6275072 | bytes 8716288 | tf_op jit(solution)/shard_map/while/body/eval_jaxpr/htk,hsk,htsk->hts/dot_general | solution.py:57
  326.4 1.7 exponential_select_fusion.2
  328.1 7.3 %fusion.136 = f32[4,64,64]{1,2,0:T(8,128)S(1)} fusion(f32[4,64,64,128]{3,2,1,0:T(8,128)S(1)} %exponential_select_fusion.2, f32[4,128,64]{1,2,0:T(8,128)S(1)} %dynamic-slice_bitcast_fusion.9, f32[4,128,64]{1,2,0:T(8,128)S(1)} %get-tuple-element.298), kind=kLoop, calls=%fused_computation.4.clone.1 | loop fusion | flops 6275072 | bytes 8716288 | tf_op jit(solution)/shard_map/while/body/eval_jaxpr/htk,hsk,htsk->hts/dot_general | solution.py:57
  338.4 1.7 exponential_select_fusion.2
  340.1 7.3 %fusion.136 = f32[4,64,64]{1,2,0:T(8,128)S(1)} fusion(f32[4,64,64,128]{3,2,1,0:T(8,128)S(1)} %exponential_select_fusion.2, f32[4,128,64]{1,2,0:T(8,128)S(1)} %dynamic-slice_bitcast_fusion.9, f32[4,128,64]{1,2,0:T(8,128)S(1)} %get-tuple-element.298), kind=kLoop, calls=%fused_computation.4.clone.1 | loop fusion | flops 6275072 | bytes 8716288 | tf_op jit(solution)/shard_map/while/body/eval_jaxpr/htk,hsk,htsk->hts/dot_general | solution.py:57
  352.6 2.3 collective-permute-start
  355.0 3.0 copy.58
  358.5 19.4 %all-gather.3 = f32[16,4,128]{2,1,0:T(4,128)S(1)} all-gather(f32[1,4,128]{2,1,0:T(4,128)S(1)} %exponential_bitcast_fusion), channel_id=2, replica_groups=mesh['sp'=16,'tp'=2] {'sp'}, dimensions={0}, use_global_device_ids=true | all-gather | bytes 34816 | tf_op jit(solution)/shard_map/all_gather | solution.py:19
  377.9 1.7 fusion.103
  379.9 20.4 %all-gather.31.cloned.1.call-done = f32[64,128,128]{2,1,0:T(8,128)} async-done(((f32[4,128,128]{2,1,0:T(8,128)}), f32[64,128,128]{2,1,0:T(8,128)}) %all-gather.31.cloned.1.call-update) | async-done | bytes 4194320 | tf_op jit(solution)/shard_map/all_gather | solution.py:19
  400.3 1.9 multiply_reduce_fusion
  404.5 37.4 %all-gather.29.cloned.1.call-done = bf16[512,2048]{1,0:T(8,128)(2,1)} async-done(((bf16[512,128]{1,0:T(8,128)(2,1)}), bf16[512,2048]{1,0:T(8,128)(2,1)}) %all-gather.29.cloned.1.call-update) | async-done | bytes 2097168 | tf_op jit(solution)/shard_map/all_gather | solution.py:179
  441.9 3.8 fusion.30
  445.8 19.6 %reduce-scatter.2.cloned.1.call-done = bf16[128,2048]{1,0:T(8,128)(2,1)} async-done(((bf16[256,2048]{1,0:T(8,128)(2,1)}), bf16[128,2048]{1,0:T(8,128)(2,1)}) %reduce-scatter.2.cloned.1.call-update) | async-done | bytes 524304 | tf_op jit(solution)/shard_map/reduce_scatter | solution.py:183
  466.7 2.0 fusion.39
  (124 shorter events, 31.2 us)
Async XLA Ops:
  6.5 371.4 %copy-start = (bf16[4,128,128]{2,1,0:T(8,128)(2,1)S(1)}, bf16[4,128,128]{2,1,0:T(8,128)(2,1)}, u32[]{:S(2)}) copy-start(bf16[4,128,128]{2,1,0:T(8,128)(2,1)} %param.31) | copy-start | bytes 393220
  6.5 26.4 %all-gather.15.cloned.1.call-start = ((), (), s32[]{:S(2)}) async-start(), calls=%async_computation.1 | async-start | bytes 1572864 | tf_op jit(solution)/shard_map/all_gather | solution.py:109
  7.3 69.3 %all-gather.17.cloned.1.call-start = ((), (), s32[]{:S(2)}) async-start(), calls=%async_computation.2 | async-start | bytes 2228224 | tf_op jit(solution)/shard_map/all_gather | solution.py:98
  8.0 110.9 %all-gather.19.cloned.1.call-start = ((), (), s32[]{:S(2)}) async-start(), calls=%async_computation.3 | async-start | bytes 2228224 | tf_op jit(solution)/shard_map/all_gather | solution.py:99
  8.7 152.4 %all-gather.21.cloned.1.call-start = ((), (), s32[]{:S(2)}) async-start(), calls=%async_computation.4 | async-start | bytes 2228224 | tf_op jit(solution)/shard_map/all_gather | solution.py:100
  9.3 194.1 %all-gather.23.cloned.1.call-start = ((), (), s32[]{:S(2)}) async-start(), calls=%async_computation.5 | async-start | bytes 2228224 | tf_op jit(solution)/shard_map/all_gather | solution.py:101
  9.9 235.7 %all-gather.25.cloned.1.call-start = ((), (), s32[]{:S(2)}) async-start(), calls=%async_computation.6 | async-start | bytes 2228224 | tf_op jit(solution)/shard_map/all_gather | solution.py:102
  10.5 277.5 %all-gather.27.cloned.1.call-start = ((), (), s32[]{:S(2)}) async-start(), calls=%async_computation.7 | async-start | bytes 2228224 | tf_op jit(solution)/shard_map/all_gather | solution.py:103
  11.2 343.7 %all-gather.33.cloned.1.call-start = ((), (), s32[]{:S(2)}) async-start(), calls=%async_computation.11 | async-start | bytes 2228224 | tf_op jit(solution)/shard_map/all_gather | solution.py:13
  12.0 388.3 %all-gather.31.cloned.1.call-start = ((), (), s32[]{:S(2)}) async-start(), calls=%async_computation.10 | async-start | bytes 4456448 | tf_op jit(solution)/shard_map/all_gather | solution.py:19
  206.5 84.7 %copy-start.3 = (bf16[256,2048]{1,0:T(8,128)(2,1)S(1)}, bf16[256,2048]{1,0:T(8,128)(2,1)}, u32[]{:S(2)}) copy-start(bf16[256,2048]{1,0:T(8,128)(2,1)} %all-gather.15.cloned.1.call-done) | copy-start | bytes 3145732
  206.5 84.7 %copy-start.8 = (f32[2048]{0:T(1024)S(1)}, f32[2048]{0:T(1024)}, u32[]{:S(2)}) copy-start(f32[2048]{0:T(1024)} %param.21) | copy-start | bytes 24580
  299.2 1.7 copy-start.2
  350.2 0.7 copy-start.1
  351.0 90.9 %all-gather.29.cloned.1.call-start = ((), (), s32[]{:S(2)}) async-start(), calls=%async_computation.8 | async-start | bytes 2228224 | tf_op jit(solution)/shard_map/all_gather | solution.py:179
  351.6 113.8 %reduce-scatter.2.cloned.1.call-start = ((), (), s32[]{:S(2)}) async-start(), calls=%async_computation.9 | async-start | bytes 1572864 | tf_op jit(solution)/shard_map/reduce_scatter | solution.py:183
  352.6 25.3 %collective-permute-start = (bf16[16,512]{1,0:T(8,128)(2,1)S(1)}, bf16[16,512]{1,0:T(8,128)(2,1)S(1)}, u32[]{:S(2)}, u32[]{:S(2)}) collective-permute-start(bf16[16,512]{1,0:T(8,128)(2,1)S(1)} %slice.99), channel_id=1, source_target_pairs={{0,2},{2,4},{4,6},{6,8},{8,10},{10,12},{12,14},{14,16},{16,18},{18... | collective-permute-start | bytes 49160 | tf_op jit(solution)/shard_map/ppermute | solution.py:33
  355.0 23.0 %copy-start.4 = (f32[256,512]{1,0:T(8,128)S(1)}, f32[256,512]{1,0:T(8,128)}, u32[]{:S(2)}) copy-start(f32[256,512]{1,0:T(8,128)} %get-tuple-element.180) | copy-start | bytes 1572868
  379.9 23.2 %copy-start.6 = (f32[512]{0:T(512)S(1)}, f32[512]{0:T(512)}, u32[]{:S(2)}) copy-start(f32[512]{0:T(512)} %param.30) | copy-start | bytes 6148
  379.9 23.2 %copy-start.7 = (f32[512]{0:T(512)S(1)}, f32[512]{0:T(512)}, u32[]{:S(2)}) copy-start(f32[512]{0:T(512)} %param.32) | copy-start | bytes 6148
  441.9 24.8 %copy-start.5 = (f32[2048]{0:T(1024)S(1)}, f32[2048]{0:T(1024)}, u32[]{:S(2)}) copy-start(f32[2048]{0:T(1024)} %param.35) | copy-start | bytes 24580
Sparse Core Ops, SparseCore 0:
  8.9 23.9 all-gather.14
  35.1 41.4 all-gather.16
  78.7 40.1 all-gather.18
  121.0 40.1 all-gather.20
  163.2 40.1 all-gather.22
  205.4 40.1 all-gather.24
  247.8 40.1 all-gather.26
  290.1 40.1 all-gather.32
  351.1 49.1 all-gather.30
  402.3 39.5 all-gather.28
  445.9 19.4 reduce-scatter.1
